TPU v7x, 32 devices: a whole 2x2x4 slice. The times are simulated.
32 devices in a mesh: fs: 16 (over z, y, x), tp: 2 (over core).
Axes of the slice: x: 2, y: 2, z: 4, core: 2. Of those that a mesh axis runs over, the one named last changes fastest.
Arguments:
- tokens: bfloat16 [12288, 2048], P('fs'), may hold values from -6 to 6
- norm_gain: float32 [2048], replicated, may hold values from 0.1 to 1.9
- gate_weight: bfloat16 [2048, 5120], P('fs', 'tp'), may hold values from -0.125 to 0.125
- up_weight: bfloat16 [2048, 5120], P('fs', 'tp'), may hold values from -0.125 to 0.125
- down_weight: bfloat16 [5120, 2048], P('tp', 'fs'), may hold values from -0.078125 to 0.078125
Outputs:
- mixed: bfloat16 [12288, 2048], P(('fs', 'tp'))
All inputs are finite; a program needn't handle non-finite values.
Results may differ from a plain program's by a relative error of at most 0.014.
Values may be sent and summed in bfloat16 or wider, within the bound.
A program may use at most 128 MiB of HBM per device.

v0:
```python
import jax
import jax.numpy as jnp
from jax import lax
from jax.sharding import PartitionSpec as P


def add_rows(normed, piece):
    return jnp.dot(normed, piece, preferred_element_type=jnp.float32)


def per_device(tokens, norm_gain, gate_weight, up_weight, down_weight):
    values = tokens.astype(jnp.float32)
    scale = lax.rsqrt(jnp.mean(values * values, axis=-1, keepdims=True) + 1e-06)
    normed = (values * scale * norm_gain).astype(jnp.bfloat16)

    def add_single(piece):
        return add_rows(normed, piece)

    gate_proj = add_single(lax.all_gather(gate_weight, "fs", axis=0, tiled=True))
    up_proj = add_single(lax.all_gather(up_weight, "fs", axis=0, tiled=True))
    hidden = (jax.nn.silu(gate_proj) * up_proj).astype(jnp.bfloat16)
    down_whole = lax.all_gather(down_weight, "fs", axis=1, tiled=True)
    return lax.psum_scatter(
        jnp.dot(hidden, down_whole, preferred_element_type=jnp.float32).astype(jnp.bfloat16),
        "tp",
        scatter_dimension=0,
        tiled=True,
    )


def solution(mesh):
    in_specs = (P("fs", None), P(), P("fs", "tp"), P("fs", "tp"), P("tp", "fs"))
    out_specs = P(("fs", "tp"), None)
    return jax.shard_map(
        per_device, mesh=mesh, in_specs=in_specs, out_specs=out_specs, check_vma=False
    )
```

profile of v0, /device:TPU:0, one launch (start us, length us, event | category | flops | bytes accessed | tf_op | source)
XLA Modules:
  0.0 489.8 jit_solution(3628427633222220995)
XLA Ops:
  6.5 0.0 all-gather.4.cloned.1.call-start
  6.5 0.7 all-gather.4.cloned.1.call-update
  7.3 0.0 all-gather.6.cloned.1.call-start
  7.3 0.7 all-gather.6.cloned.1.call-update
  8.0 0.0 all-gather.8.cloned.1.call-start
  8.1 0.7 all-gather.8.cloned.1.call-update
  8.7 0.0 reduce-scatter.2.cloned.1.call-start
  8.8 2.6 fusion
  11.4 0.0 copy-start
  11.4 0.0 copy-start.1
  11.4 132.8 %all-gather.4.cloned.1.call-done = bf16[2048,2560]{1,0:T(8,128)(2,1)} async-done(((bf16[128,2560]{1,0:T(8,128)(2,1)}), bf16[2048,2560]{1,0:T(8,128)(2,1)}) %all-gather.4.cloned.1.call-update) | async-done | bytes 10485776 | tf_op jit(solution)/shard_map/all_gather | solution.py:19
  144.2 13.9 %fusion.5 = f32[768,2560]{1,0:T(8,128)} fusion(bf16[2048,2560]{1,0:T(8,128)(2,1)} %all-gather.4.cloned.1.call-done, bf16[768,2048]{1,0:T(8,128)(2,1)} %param.5, f32[2048]{0:T(1024)} %param.6, f32[768]{0:T(1024)S(1)} %add_rsqrt_fusion), kind=kOutput, calls=%fused_computation.7 | convolution fusion | flops 8059355136 | bytes 21507072 | tf_op jit(solution)/shard_map/dot_general | solution.py:8
  158.2 118.4 %all-gather.6.cloned.1.call-done = bf16[2048,2560]{1,0:T(8,128)(2,1)} async-done(((bf16[128,2560]{1,0:T(8,128)(2,1)}), bf16[2048,2560]{1,0:T(8,128)(2,1)}) %all-gather.6.cloned.1.call-update) | async-done | bytes 10485776 | tf_op jit(solution)/shard_map/all_gather | solution.py:20
  276.6 169.6 %all-gather.8.cloned.1.call-done = bf16[2560,2048]{1,0:T(8,128)(2,1)} async-done(((bf16[2560,128]{1,0:T(8,128)(2,1)}), bf16[2560,2048]{1,0:T(8,128)(2,1)}) %all-gather.8.cloned.1.call-update) | async-done | bytes 10485776 | tf_op jit(solution)/shard_map/all_gather | solution.py:22
  446.2 0.0 copy-done
  446.2 0.0 copy-done.1
  446.2 27.6 %convolution_convert_fusion = bf16[768,2048]{1,0:T(8,128)(2,1)} fusion(bf16[2560,2048]{1,0:T(8,128)(2,1)} %all-gather.8.cloned.1.call-done, f32[768,2560]{1,0:T(8,128)} %fusion.5, bf16[2048,2560]{1,0:T(8,128)(2,1)} %all-gather.6.cloned.1.call-done, bf16[768,2048]{1,0:T(8,128)(2,1)S(1)} %copy-done, f32[2048]{0:T(1024)S(1)} %copy-done.1, ...), kind=kOutput, calls=%fused_computation.6 | convolution fusion | flops 16125788160 | bytes 35138560 | tf_op jit(solution)/shard_map/dot_general | solution.py:24
  473.8 0.0 reduce-scatter.2.cloned.1.call-update
  473.8 9.5 %reduce-scatter.2.cloned.1.call-done = bf16[384,2048]{1,0:T(8,128)(2,1)} async-done(((bf16[768,2048]{1,0:T(8,128)(2,1)}), bf16[384,2048]{1,0:T(8,128)(2,1)}) %reduce-scatter.2.cloned.1.call-update) | async-done | bytes 1572880 | tf_op jit(solution)/shard_map/reduce_scatter | solution.py:23
  (1 shorter events, 0.0 us)
Async XLA Ops:
  6.5 137.7 %all-gather.4.cloned.1.call-start = ((), (), s32[]{:S(2)}) async-start(), calls=%async_computation.1 | async-start | bytes 11141120 | tf_op jit(solution)/shard_map/all_gather | solution.py:19
  7.3 269.4 %all-gather.6.cloned.1.call-start = ((), (), s32[]{:S(2)}) async-start(), calls=%async_computation.2 | async-start | bytes 11141120 | tf_op jit(solution)/shard_map/all_gather | solution.py:20
  8.0 438.2 %all-gather.8.cloned.1.call-start = ((), (), s32[]{:S(2)}) async-start(), calls=%async_computation.3 | async-start | bytes 11141120 | tf_op jit(solution)/shard_map/all_gather | solution.py:22
  8.7 474.6 %reduce-scatter.2.cloned.1.call-start = ((), (), s32[]{:S(2)}) async-start(), calls=%async_computation.4 | async-start | bytes 4718592 | tf_op jit(solution)/shard_map/reduce_scatter | solution.py:23
  11.4 434.8 %copy-start = (bf16[768,2048]{1,0:T(8,128)(2,1)S(1)}, bf16[768,2048]{1,0:T(8,128)(2,1)}, u32[]{:S(2)}) copy-start(bf16[768,2048]{1,0:T(8,128)(2,1)} %param.5) | copy-start | bytes 9437188
  11.4 434.8 %copy-start.1 = (f32[2048]{0:T(1024)S(1)}, f32[2048]{0:T(1024)}, u32[]{:S(2)}) copy-start(f32[2048]{0:T(1024)} %param.6) | copy-start | bytes 24580
Sparse Core Ops, SparseCore 0:
  10.0 134.1 all-gather.3
  146.9 129.6 all-gather.5
  279.3 166.8 all-gather.7
  473.9 9.3 reduce-scatter.1
where the time goes:
time: 490 us
  waiting for transfers between devices  432 us (88%)
  matrix products  41.5 us (8%)
  between operations  13.1 us (3%)
    all_gather x1, waiting for transfers between devices, per_device(): down_whole = lax.all_gather(down_weight, 'fs', axis=1, tiled=True)  170 us
    all_gather x1, waiting for transfers between devices, per_device(): lax.all_gather(gate_weight, 'fs', axis=0, tiled=True)  133 us
    all_gather x1, waiting for transfers between devices, per_device(): up_proj = add_single(lax.all_gather(up_weight, 'fs', axis=0, tiled=True))  118 us
    dot_general x1, matrix products, per_device(): jnp.dot(hidden, down_whole, preferred_element_type=jnp.float32)  27.6 us
    dot_general x1, matrix products, add_rows(): return jnp.dot(normed, piece, preferred_element_type=jnp.float32)  13.9 us
  transfers between devices with their start and end apart: 4, of which 4 were waited for; matrix products, arithmetic and copies ran while one was open for 3% of the time, Pallas kernels for 0%

commit v1 on v0

--- a/solution.py
+++ b/solution.py
@@ -19,7 +19,12 @@
     gate_proj = add_single(lax.all_gather(gate_weight, "fs", axis=0, tiled=True))
     up_proj = add_single(lax.all_gather(up_weight, "fs", axis=0, tiled=True))
     hidden = (jax.nn.silu(gate_proj) * up_proj).astype(jnp.bfloat16)
-    down_whole = lax.all_gather(down_weight, "fs", axis=1, tiled=True)
+    ring = [down_weight]
+    for hop in range(15):
+        ring.append(lax.ppermute(ring[-1], "fs", [(dev, (dev + 1) % 16) for dev in range(16)]))
+    down_whole = jnp.roll(
+        jnp.concatenate(ring[::-1], axis=1), (lax.axis_index("fs") + 1) * ring[0].shape[1], axis=1
+    )
     return lax.psum_scatter(
         jnp.dot(hidden, down_whole, preferred_element_type=jnp.float32).astype(jnp.bfloat16),
         "tp",

time: 490 us -> 553 us (1.13)
  local copies, waits for them, and re-layouts: 0.01 us -> 56.7 us
    ppermute x0 -> x15, waiting for transfers between devices: none -> 412 us  [per_device(): lax.ppermute(ring[-1], 'fs', [(dev, (dev + 1) % 16) for dev in range(16)])]
    all_gather x1 -> x0, waiting for transfers between devices: 170 us -> none  [per_device(): down_whole = lax.all_gather(down_weight, 'fs', axis=1, tiled=True)]
    all_gather x1, waiting for transfers between devices: 133 us -> 0.01 us  [per_device(): lax.all_gather(gate_weight, 'fs', axis=0, tiled=True)]
    all_gather x1, waiting for transfers between devices: 118 us -> 0.01 us  [per_device(): up_proj = add_single(lax.all_gather(up_weight, 'fs', axis=0, tiled=True))]
    unnamed x4 -> x89, local copies, waits for them, and re-layouts: 0.01 us -> 55.8 us
    dot_general x1, matrix products: 27.6 us -> 12.3 us  [per_device(): jnp.dot(hidden, down_whole, preferred_element_type=jnp.float32)]
    reduce_scatter x1, waiting for transfers between devices: 9.51 us -> 24.1 us  [per_device(): lax.psum_scatter(jnp.dot(hidden, down_whole, preferred_element_type=jnp.f...]
    dot_general x1 -> x2, matrix products: 13.9 us -> 26.8 us  [add_rows(): return jnp.dot(normed, piece, preferred_element_type=jnp.float32)]
  transfers between devices with their start and end apart: 4 -> 18, of which waited for: 4 -> 16; matrix products, arithmetic and copies ran while one was open for 3% -> 11% of each run, Pallas kernels for 0% -> 0%
where the time goes in v1:
time: 553 us; the launch traced here: 552 us
  waiting for transfers between devices  437 us (79%)
  local copies, waits for them, and re-layouts  56.7 us (10%)
  matrix products  39.1 us (7%)
  between operations  13.3 us (2%)
    ppermute x15, waiting for transfers between devices, per_device(): lax.ppermute(ring[-1], 'fs', [(dev, (dev + 1) % 16) for dev in range(16)])  412 us
    unnamed x89, local copies, waits for them, and re-layouts  55.8 us
    dot_general x2, matrix products, add_rows(): return jnp.dot(normed, piece, preferred_element_type=jnp.float32)  26.8 us
    reduce_scatter x1, waiting for transfers between devices, per_device(): lax.psum_scatter(jnp.dot(hidden, down_whole, preferred_element_type=jnp.f...  24.1 us
    dot_general x1, matrix products, per_device(): jnp.dot(hidden, down_whole, preferred_element_type=jnp.float32)  12.3 us
  transfers between devices with their start and end apart: 18, of which 16 were waited for; matrix products, arithmetic and copies ran while one was open for 11% of the time, Pallas kernels for 0%

profile of v1, /device:TPU:0, one launch (start us, length us, event | category | flops | bytes accessed | tf_op | source)
XLA Modules:
  0.0 552.4 jit_solution(17626052501318226953)
XLA Ops:
  7.3 3.0 collective-permute-start
  10.3 20.8 %collective-permute-done = bf16[2560,128]{1,0:T(8,128)(2,1)S(1)} collective-permute-done((bf16[2560,128]{1,0:T(8,128)(2,1)}, bf16[2560,128]{1,0:T(8,128)(2,1)S(1)}, u32[]{:S(2)}, u32[]{:S(2)}) %collective-permute-start) | collective-permute-done | bytes 655392 | tf_op jit(solution)/shard_map/ppermute | solution.py:24
  32.0 25.5 %collective-permute-done.1 = bf16[2560,128]{1,0:T(8,128)(2,1)S(1)} collective-permute-done((bf16[2560,128]{1,0:T(8,128)(2,1)S(1)}, bf16[2560,128]{1,0:T(8,128)(2,1)S(1)}, u32[]{:S(2)}, u32[]{:S(2)}) %collective-permute-start.1) | collective-permute-done | bytes 655392 | tf_op jit(solution)/shard_map/ppermute | solution.py:24
  58.4 32.1 %collective-permute-done.2 = bf16[2560,128]{1,0:T(8,128)(2,1)S(1)} collective-permute-done((bf16[2560,128]{1,0:T(8,128)(2,1)S(1)}, bf16[2560,128]{1,0:T(8,128)(2,1)S(1)}, u32[]{:S(2)}, u32[]{:S(2)}) %collective-permute-start.2) | collective-permute-done | bytes 655392 | tf_op jit(solution)/shard_map/ppermute | solution.py:24
  91.3 25.6 %collective-permute-done.3 = bf16[2560,128]{1,0:T(8,128)(2,1)S(1)} collective-permute-done((bf16[2560,128]{1,0:T(8,128)(2,1)S(1)}, bf16[2560,128]{1,0:T(8,128)(2,1)S(1)}, u32[]{:S(2)}, u32[]{:S(2)}) %collective-permute-start.3) | collective-permute-done | bytes 655392 | tf_op jit(solution)/shard_map/ppermute | solution.py:24
  117.7 34.3 %collective-permute-done.4 = bf16[2560,128]{1,0:T(8,128)(2,1)S(1)} collective-permute-done((bf16[2560,128]{1,0:T(8,128)(2,1)S(1)}, bf16[2560,128]{1,0:T(8,128)(2,1)S(1)}, u32[]{:S(2)}, u32[]{:S(2)}) %collective-permute-start.4) | collective-permute-done | bytes 655392 | tf_op jit(solution)/shard_map/ppermute | solution.py:24
  152.1 29.4 %collective-permute-done.5 = bf16[2560,128]{1,0:T(8,128)(2,1)S(1)} collective-permute-done((bf16[2560,128]{1,0:T(8,128)(2,1)S(1)}, bf16[2560,128]{1,0:T(8,128)(2,1)S(1)}, u32[]{:S(2)}, u32[]{:S(2)}) %collective-permute-start.5) | collective-permute-done | bytes 655392 | tf_op jit(solution)/shard_map/ppermute | solution.py:24
  181.5 32.6 %collective-permute-done.6 = bf16[2560,128]{1,0:T(8,128)(2,1)S(1)} collective-permute-done((bf16[2560,128]{1,0:T(8,128)(2,1)S(1)}, bf16[2560,128]{1,0:T(8,128)(2,1)S(1)}, u32[]{:S(2)}, u32[]{:S(2)}) %collective-permute-start.6) | collective-permute-done | bytes 655392 | tf_op jit(solution)/shard_map/ppermute | solution.py:24
  214.9 26.8 %collective-permute-done.7 = bf16[2560,128]{1,0:T(8,128)(2,1)S(1)} collective-permute-done((bf16[2560,128]{1,0:T(8,128)(2,1)S(1)}, bf16[2560,128]{1,0:T(8,128)(2,1)S(1)}, u32[]{:S(2)}, u32[]{:S(2)}) %collective-permute-start.7) | collective-permute-done | bytes 655392 | tf_op jit(solution)/shard_map/ppermute | solution.py:24
  242.6 24.0 %collective-permute-done.8 = bf16[2560,128]{1,0:T(8,128)(2,1)S(1)} collective-permute-done((bf16[2560,128]{1,0:T(8,128)(2,1)S(1)}, bf16[2560,128]{1,0:T(8,128)(2,1)S(1)}, u32[]{:S(2)}, u32[]{:S(2)}) %collective-permute-start.8) | collective-permute-done | bytes 655392 | tf_op jit(solution)/shard_map/ppermute | solution.py:24
  267.5 31.5 %collective-permute-done.9 = bf16[2560,128]{1,0:T(8,128)(2,1)S(1)} collective-permute-done((bf16[2560,128]{1,0:T(8,128)(2,1)S(1)}, bf16[2560,128]{1,0:T(8,128)(2,1)S(1)}, u32[]{:S(2)}, u32[]{:S(2)}) %collective-permute-start.9) | collective-permute-done | bytes 655392 | tf_op jit(solution)/shard_map/ppermute | solution.py:24
  299.8 22.3 %collective-permute-done.10 = bf16[2560,128]{1,0:T(8,128)(2,1)S(1)} collective-permute-done((bf16[2560,128]{1,0:T(8,128)(2,1)S(1)}, bf16[2560,128]{1,0:T(8,128)(2,1)S(1)}, u32[]{:S(2)}, u32[]{:S(2)}) %collective-permute-start.10) | collective-permute-done | bytes 655392 | tf_op jit(solution)/shard_map/ppermute | solution.py:24
  323.0 33.0 %collective-permute-done.11 = bf16[2560,128]{1,0:T(8,128)(2,1)S(1)} collective-permute-done((bf16[2560,128]{1,0:T(8,128)(2,1)S(1)}, bf16[2560,128]{1,0:T(8,128)(2,1)S(1)}, u32[]{:S(2)}, u32[]{:S(2)}) %collective-permute-start.11) | collective-permute-done | bytes 655392 | tf_op jit(solution)/shard_map/ppermute | solution.py:24
  356.9 32.9 %collective-permute-done.12 = bf16[2560,128]{1,0:T(8,128)(2,1)S(1)} collective-permute-done((bf16[2560,128]{1,0:T(8,128)(2,1)S(1)}, bf16[2560,128]{1,0:T(8,128)(2,1)S(1)}, u32[]{:S(2)}, u32[]{:S(2)}) %collective-permute-start.12) | collective-permute-done | bytes 655392 | tf_op jit(solution)/shard_map/ppermute | solution.py:24
  390.6 26.7 %collective-permute-done.13 = bf16[2560,128]{1,0:T(8,128)(2,1)} collective-permute-done((bf16[2560,128]{1,0:T(8,128)(2,1)S(1)}, bf16[2560,128]{1,0:T(8,128)(2,1)}, u32[]{:S(2)}, u32[]{:S(2)}) %collective-permute-start.13) | collective-permute-done | bytes 655392 | tf_op jit(solution)/shard_map/ppermute | solution.py:24
  417.4 2.7 fusion.2
  420.2 15.0 %collective-permute-done.14 = bf16[2560,128]{1,0:T(8,128)(2,1)} collective-permute-done((bf16[2560,128]{1,0:T(8,128)(2,1)}, bf16[2560,128]{1,0:T(8,128)(2,1)}, u32[]{:S(2)}, u32[]{:S(2)}) %collective-permute-start.14) | collective-permute-done | bytes 655392 | tf_op jit(solution)/shard_map/ppermute | solution.py:24
  435.2 2.1 constant_dynamic-update-slice_fusion.31
  441.3 2.0 constant_dynamic-update-slice_fusion.28
  467.4 2.1 constant_dynamic-update-slice_fusion.14
  482.6 13.0 %fusion.9 = f32[768,2560]{1,0:T(8,128)} fusion(bf16[2048,2560]{1,0:T(8,128)(2,1)} %all-gather.3.cloned.1.call-done, bf16[768,2048]{1,0:T(8,128)(2,1)S(1)} %copy-done, f32[2048]{0:T(1024)S(1)} %copy-done.28, f32[768]{0:T(1024)S(1)} %add_rsqrt_fusion), kind=kOutput, calls=%fused_computation.9 | convolution fusion | flops 8059355136 | bytes 21507072 | tf_op jit(solution)/shard_map/dot_general | solution.py:8
  495.6 13.9 %multiply_convert_fusion = bf16[768,2560]{1,0:T(8,128)(2,1)S(1)} fusion(f32[768,2560]{1,0:T(8,128)} %fusion.9, bf16[2048,2560]{1,0:T(8,128)(2,1)} %all-gather.5.cloned.1.call-done, bf16[768,2048]{1,0:T(8,128)(2,1)S(1)} %copy-done, f32[2048]{0:T(1024)S(1)} %copy-done.28, f32[768]{0:T(1024)S(1)} %add_rsqrt_fusion), kind=kOutput, calls=%fused_computation.2 | convolution fusion | flops 8071151616 | bytes 25439232 | tf_op jit(solution)/shard_map/dot_general | solution.py:8
  509.4 12.3 %fusion.5 = bf16[768,2048]{1,0:T(8,128)(2,1)} fusion(bf16[768,2560]{1,0:T(8,128)(2,1)S(1)} %multiply_convert_fusion, bf16[2560,4096]{1,0:T(8,128)(2,1)} %constant_dynamic-update-slice_fusion, s32[]{:T(128)S(6)} %select_n.14), kind=kOutput, calls=%fused_computation.8 | convolution fusion | flops 8054636544 | bytes 17563652 | tf_op jit(solution)/shard_map/dot_general | solution.py:29
  521.7 24.1 %reduce-scatter.2.cloned.1.call-done = bf16[384,2048]{1,0:T(8,128)(2,1)} async-done(((bf16[768,2048]{1,0:T(8,128)(2,1)}), bf16[384,2048]{1,0:T(8,128)(2,1)}) %reduce-scatter.2.cloned.1.call-update) | async-done | bytes 1572880 | tf_op jit(solution)/shard_map/reduce_scatter | solution.py:28
  (110 shorter events, 51.4 us)
Async XLA Ops:
  6.5 476.0 %all-gather.3.cloned.1.call-start = ((), (), s32[]{:S(2)}) async-start(), calls=%async_computation.1 | async-start | bytes 11141120 | tf_op jit(solution)/shard_map/all_gather | solution.py:19
  7.3 488.3 %all-gather.5.cloned.1.call-start = ((), (), s32[]{:S(2)}) async-start(), calls=%async_computation.2 | async-start | bytes 11141120 | tf_op jit(solution)/shard_map/all_gather | solution.py:20
  7.3 23.8 %collective-permute-start = (bf16[2560,128]{1,0:T(8,128)(2,1)}, bf16[2560,128]{1,0:T(8,128)(2,1)S(1)}, u32[]{:S(2)}, u32[]{:S(2)}) collective-permute-start(bf16[2560,128]{1,0:T(8,128)(2,1)} %param.9), channel_id=1, source_target_pairs={{0,2},{2,4},{4,6},{6,8},{8,10},{10,12},{12,14},{14,16},{16,18},{18... | collective-permute-start | bytes 1966088 | tf_op jit(solution)/shard_map/ppermute | solution.py:24
  32.0 25.5 %collective-permute-start.1 = (bf16[2560,128]{1,0:T(8,128)(2,1)S(1)}, bf16[2560,128]{1,0:T(8,128)(2,1)S(1)}, u32[]{:S(2)}, u32[]{:S(2)}) collective-permute-start(bf16[2560,128]{1,0:T(8,128)(2,1)S(1)} %collective-permute-done), channel_id=1, source_target_pairs={{0,2},{2,4},{4,6},{6,8},{8,10},{10,12},{12,14},{14,16},{16,18},{18... | collective-permute-start | bytes 1966088 | tf_op jit(solution)/shard_map/ppermute | solution.py:24
  58.3 32.1 %collective-permute-start.2 = (bf16[2560,128]{1,0:T(8,128)(2,1)S(1)}, bf16[2560,128]{1,0:T(8,128)(2,1)S(1)}, u32[]{:S(2)}, u32[]{:S(2)}) collective-permute-start(bf16[2560,128]{1,0:T(8,128)(2,1)S(1)} %collective-permute-done.1), channel_id=1, source_target_pairs={{0,2},{2,4},{4,6},{6,8},{8,10},{10,12},{12,14},{14,16},{16,18},{18... | collective-permute-start | bytes 1966088 | tf_op jit(solution)/shard_map/ppermute | solution.py:24
  91.3 25.6 %collective-permute-start.3 = (bf16[2560,128]{1,0:T(8,128)(2,1)S(1)}, bf16[2560,128]{1,0:T(8,128)(2,1)S(1)}, u32[]{:S(2)}, u32[]{:S(2)}) collective-permute-start(bf16[2560,128]{1,0:T(8,128)(2,1)S(1)} %collective-permute-done.2), channel_id=1, source_target_pairs={{0,2},{2,4},{4,6},{6,8},{8,10},{10,12},{12,14},{14,16},{16,18},{18... | collective-permute-start | bytes 1966088 | tf_op jit(solution)/shard_map/ppermute | solution.py:24
  117.7 34.3 %collective-permute-start.4 = (bf16[2560,128]{1,0:T(8,128)(2,1)S(1)}, bf16[2560,128]{1,0:T(8,128)(2,1)S(1)}, u32[]{:S(2)}, u32[]{:S(2)}) collective-permute-start(bf16[2560,128]{1,0:T(8,128)(2,1)S(1)} %collective-permute-done.3), channel_id=1, source_target_pairs={{0,2},{2,4},{4,6},{6,8},{8,10},{10,12},{12,14},{14,16},{16,18},{18... | collective-permute-start | bytes 1966088 | tf_op jit(solution)/shard_map/ppermute | solution.py:24
  152.0 268.1 %copy-start.10 = (bf16[2560,128]{1,0:T(8,128)(2,1)}, bf16[2560,128]{1,0:T(8,128)(2,1)S(1)}, u32[]{:S(2)}) copy-start(bf16[2560,128]{1,0:T(8,128)(2,1)S(1)} %collective-permute-done.4) | copy-start | bytes 1966084
  152.0 29.5 %collective-permute-start.5 = (bf16[2560,128]{1,0:T(8,128)(2,1)S(1)}, bf16[2560,128]{1,0:T(8,128)(2,1)S(1)}, u32[]{:S(2)}, u32[]{:S(2)}) collective-permute-start(bf16[2560,128]{1,0:T(8,128)(2,1)S(1)} %collective-permute-done.4), channel_id=1, source_target_pairs={{0,2},{2,4},{4,6},{6,8},{8,10},{10,12},{12,14},{14,16},{16,18},{18... | collective-permute-start | bytes 1966088 | tf_op jit(solution)/shard_map/ppermute | solution.py:24
  152.1 393.8 %reduce-scatter.2.cloned.1.call-start = ((), (), s32[]{:S(2)}) async-start(), calls=%async_computation.3 | async-start | bytes 4718592 | tf_op jit(solution)/shard_map/reduce_scatter | solution.py:28
  181.5 238.6 %copy-start.12 = (bf16[2560,128]{1,0:T(8,128)(2,1)}, bf16[2560,128]{1,0:T(8,128)(2,1)S(1)}, u32[]{:S(2)}) copy-start(bf16[2560,128]{1,0:T(8,128)(2,1)S(1)} %collective-permute-done.5) | copy-start | bytes 1966084
  181.5 32.6 %collective-permute-start.6 = (bf16[2560,128]{1,0:T(8,128)(2,1)S(1)}, bf16[2560,128]{1,0:T(8,128)(2,1)S(1)}, u32[]{:S(2)}, u32[]{:S(2)}) collective-permute-start(bf16[2560,128]{1,0:T(8,128)(2,1)S(1)} %collective-permute-done.5), channel_id=1, source_target_pairs={{0,2},{2,4},{4,6},{6,8},{8,10},{10,12},{12,14},{14,16},{16,18},{18... | collective-permute-start | bytes 1966088 | tf_op jit(solution)/shard_map/ppermute | solution.py:24
  214.9 26.8 %collective-permute-start.7 = (bf16[2560,128]{1,0:T(8,128)(2,1)S(1)}, bf16[2560,128]{1,0:T(8,128)(2,1)S(1)}, u32[]{:S(2)}, u32[]{:S(2)}) collective-permute-start(bf16[2560,128]{1,0:T(8,128)(2,1)S(1)} %collective-permute-done.6), channel_id=1, source_target_pairs={{0,2},{2,4},{4,6},{6,8},{8,10},{10,12},{12,14},{14,16},{16,18},{18... | collective-permute-start | bytes 1966088 | tf_op jit(solution)/shard_map/ppermute | solution.py:24
  242.5 24.0 %collective-permute-start.8 = (bf16[2560,128]{1,0:T(8,128)(2,1)S(1)}, bf16[2560,128]{1,0:T(8,128)(2,1)S(1)}, u32[]{:S(2)}, u32[]{:S(2)}) collective-permute-start(bf16[2560,128]{1,0:T(8,128)(2,1)S(1)} %collective-permute-done.7), channel_id=1, source_target_pairs={{0,2},{2,4},{4,6},{6,8},{8,10},{10,12},{12,14},{14,16},{16,18},{18... | collective-permute-start | bytes 1966088 | tf_op jit(solution)/shard_map/ppermute | solution.py:24
  267.5 31.5 %collective-permute-start.9 = (bf16[2560,128]{1,0:T(8,128)(2,1)S(1)}, bf16[2560,128]{1,0:T(8,128)(2,1)S(1)}, u32[]{:S(2)}, u32[]{:S(2)}) collective-permute-start(bf16[2560,128]{1,0:T(8,128)(2,1)S(1)} %collective-permute-done.8), channel_id=1, source_target_pairs={{0,2},{2,4},{4,6},{6,8},{8,10},{10,12},{12,14},{14,16},{16,18},{18... | collective-permute-start | bytes 1966088 | tf_op jit(solution)/shard_map/ppermute | solution.py:24
  299.8 22.3 %collective-permute-start.10 = (bf16[2560,128]{1,0:T(8,128)(2,1)S(1)}, bf16[2560,128]{1,0:T(8,128)(2,1)S(1)}, u32[]{:S(2)}, u32[]{:S(2)}) collective-permute-start(bf16[2560,128]{1,0:T(8,128)(2,1)S(1)} %collective-permute-done.9), channel_id=1, source_target_pairs={{0,2},{2,4},{4,6},{6,8},{8,10},{10,12},{12,14},{14,16},{16,18},{18... | collective-permute-start | bytes 1966088 | tf_op jit(solution)/shard_map/ppermute | solution.py:24
  323.0 33.0 %collective-permute-start.11 = (bf16[2560,128]{1,0:T(8,128)(2,1)S(1)}, bf16[2560,128]{1,0:T(8,128)(2,1)S(1)}, u32[]{:S(2)}, u32[]{:S(2)}) collective-permute-start(bf16[2560,128]{1,0:T(8,128)(2,1)S(1)} %collective-permute-done.10), channel_id=1, source_target_pairs={{0,2},{2,4},{4,6},{6,8},{8,10},{10,12},{12,14},{14,16},{16,18},{18... | collective-permute-start | bytes 1966088 | tf_op jit(solution)/shard_map/ppermute | solution.py:24
  356.9 32.9 %collective-permute-start.12 = (bf16[2560,128]{1,0:T(8,128)(2,1)S(1)}, bf16[2560,128]{1,0:T(8,128)(2,1)S(1)}, u32[]{:S(2)}, u32[]{:S(2)}) collective-permute-start(bf16[2560,128]{1,0:T(8,128)(2,1)S(1)} %collective-permute-done.11), channel_id=1, source_target_pairs={{0,2},{2,4},{4,6},{6,8},{8,10},{10,12},{12,14},{14,16},{16,18},{18... | collective-permute-start | bytes 1966088 | tf_op jit(solution)/shard_map/ppermute | solution.py:24
  390.6 26.7 %collective-permute-start.13 = (bf16[2560,128]{1,0:T(8,128)(2,1)S(1)}, bf16[2560,128]{1,0:T(8,128)(2,1)}, u32[]{:S(2)}, u32[]{:S(2)}) collective-permute-start(bf16[2560,128]{1,0:T(8,128)(2,1)S(1)} %collective-permute-done.12), channel_id=1, source_target_pairs={{0,2},{2,4},{4,6},{6,8},{8,10},{10,12},{12,14},{14,16},{16,18},{18... | collective-permute-start | bytes 1966088 | tf_op jit(solution)/shard_map/ppermute | solution.py:24
  417.3 17.9 %collective-permute-start.14 = (bf16[2560,128]{1,0:T(8,128)(2,1)}, bf16[2560,128]{1,0:T(8,128)(2,1)}, u32[]{:S(2)}, u32[]{:S(2)}) collective-permute-start(bf16[2560,128]{1,0:T(8,128)(2,1)} %collective-permute-done.13), channel_id=1, source_target_pairs={{0,2},{2,4},{4,6},{6,8},{8,10},{10,12},{12,14},{14,16},{16,18},{18... | collective-permute-start | bytes 1966088 | tf_op jit(solution)/shard_map/ppermute | solution.py:24
  417.3 61.5 %copy-start.7 = (bf16[2560,128]{1,0:T(8,128)(2,1)S(1)}, bf16[2560,128]{1,0:T(8,128)(2,1)}, u32[]{:S(2)}) copy-start(bf16[2560,128]{1,0:T(8,128)(2,1)} %copy-done.6) | copy-start | bytes 1966084
  417.4 62.4 %copy-start.5 = (bf16[2560,128]{1,0:T(8,128)(2,1)S(1)}, bf16[2560,128]{1,0:T(8,128)(2,1)}, u32[]{:S(2)}) copy-start(bf16[2560,128]{1,0:T(8,128)(2,1)} %copy-done.4) | copy-start | bytes 1966084
  420.1 62.4 %copy-start = (bf16[768,2048]{1,0:T(8,128)(2,1)S(1)}, bf16[768,2048]{1,0:T(8,128)(2,1)}, u32[]{:S(2)}) copy-start(bf16[768,2048]{1,0:T(8,128)(2,1)} %param.5) | copy-start | bytes 9437188
  420.1 62.4 %copy-start.28 = (f32[2048]{0:T(1024)S(1)}, f32[2048]{0:T(1024)}, u32[]{:S(2)}) copy-start(f32[2048]{0:T(1024)} %param.6) | copy-start | bytes 24580
  (23 other events, 660.8 us)
Sparse Core Ops, SparseCore 0:
  10.0 187.1 all-gather.2
  199.9 200.9 all-gather.4
  521.8 23.9 reduce-scatter.1
